TPU v7x, 32 devices: a whole 2x2x4 slice. The times are simulated.
32 devices in a mesh: dp: 2 (over x), kv: 8 (over z, y), tp: 2 (over core).
Axes of the slice: x: 2, y: 2, z: 4, core: 2. Of those that a mesh axis runs over, the one named last changes fastest.
Arguments:
- tokens: bfloat16 [32, 16, 4096], P('dp', None, 'kv'), may hold values from -64 to 64
- in_gain: bfloat16 [4096], P('kv'), may hold values from 0.099609375 to 1.8984375
- query_weight: bfloat16 [4096, 4096], P('kv', 'tp'), may hold values from -0.125 to 0.125
- key_weight: bfloat16 [4096, 4096], P('kv', 'tp'), may hold values from -0.125 to 0.125
- value_weight: bfloat16 [4096, 4096], P('kv', 'tp'), may hold values from -0.09375 to 0.09375
- out_weight: bfloat16 [4096, 4096], P('tp', 'kv'), may hold values from -0.1875 to 0.1875
- lambdas: float32 [16], P('tp'), may hold values from 0.3 to 0.8
- sub_gain: bfloat16 [256], replicated, may hold values from 0.099609375 to 1.8984375
- key_cache: bfloat16 [32, 256, 16, 2, 128], P('dp', 'kv', 'tp'), may hold values from -248 to 248
- value_cache: bfloat16 [32, 256, 16, 256], P('dp', 'kv', 'tp'), may hold values from -6 to 6
- cache_len: int32 [32], P('dp'), may hold values from 128 to 224
- accepted: int32 [32], P('dp'), may hold values from 0 to 16
- parents: int32 [32, 16], P('dp'), may hold values from -1 to 14, as said below
Outputs:
- output: bfloat16 [32, 16, 4096], P('dp', None, ('kv', 'tp'))
- key_cache_out: bfloat16 [32, 256, 16, 2, 128], P('dp', 'kv', 'tp')
- value_cache_out: bfloat16 [32, 256, 16, 256], P('dp', 'kv', 'tp')
Inputs may be any that keep to these rules, and one draw needn't show every extreme that they name: `parents`: each proposal's parent is -1 (the text already in the cache) or one of the three proposals just before it; the last proposal's parent is the one just before it. Positions below cache_len plus accepted hold a sequence's text; the later ones are stale.
All inputs are finite; a program needn't handle non-finite values.
Results may differ from a plain program's by a relative error of at most 0.019.
The roundings to bfloat16 on the way count: a program that leaves them out, or rounds other values in their place, can miss the bound.
Values may be sent and summed in bfloat16 or wider, within the bound.
No kernel may reach another device: no remote copies, remote signals or barrier semaphores. Data moves between devices by JAX's collectives and lax.ppermute only.
A program may use at most 64 MiB of HBM per device.

v0:
```python
import math

import jax
import jax.numpy as jnp
from jax import lax
from jax.sharding import PartitionSpec as P

D = 4096


LAMBDA_SCALE = 0.2 + 0.6 * math.exp(-0.6)
NEG_FILL = -1e30


def joined(value, axis, join):
    pieces = jax.tree.map(lambda part: lax.all_gather(part, axis), value)
    head = jax.tree.map(lambda part: part[0], pieces)
    tail = jax.tree.map(lambda part: part[1:], pieces)
    total, _ = lax.scan(lambda total, share: (join(total, share), None), head, tail)
    return total


def visible_links(parents):
    number = parents.shape[-1]
    identity = jnp.eye(number, dtype=jnp.float32)
    parent_links = (parents[..., :, None] == jnp.arange(number, dtype=jnp.int32)[None, :]).astype(
        jnp.float32
    )

    def extend(repeat, reached):
        return jnp.maximum(
            identity,
            jnp.einsum("bij,bjk->bik", parent_links, reached, precision=lax.Precision.HIGHEST),
        )

    reached = lax.fori_loop(0, number, extend, jnp.broadcast_to(identity, parent_links.shape))
    depths = (jnp.sum(reached, axis=-1) - 1.0).astype(jnp.int32)
    return (reached > 0.5, depths)


def rotate(values, positions):
    half_dim = values.shape[-1] // 2
    frequency = 10000.0 ** (-jnp.arange(half_dim, dtype=jnp.float32) / half_dim)
    angles = positions.astype(jnp.float32)[..., None] * frequency
    cosine = jnp.cos(angles)[..., None, None, :]
    sine_part = jnp.sin(angles)[..., None, None, :]
    lower_half = values[..., :half_dim]
    upper_half = values[..., half_dim:]
    return jnp.concatenate(
        [
            lower_half * cosine - upper_half * sine_part,
            upper_half * cosine + lower_half * sine_part,
        ],
        axis=-1,
    )


def merge_stats(former, latter):
    highest = jnp.maximum(former[0], latter[0])
    totals = former[1] * jnp.exp(former[0] - highest) + latter[1] * jnp.exp(latter[0] - highest)
    return (highest, totals)


def per_device(
    tokens,
    in_gain,
    query_weight,
    key_weight,
    value_weight,
    out_weight,
    lambdas,
    sub_gain,
    key_cache,
    value_cache,
    cache_len,
    accepted,
    parents,
):
    seq_count, prop_count, width_part = tokens.shape
    heads_here = lambdas.shape[0]
    span_here = key_cache.shape[1]
    head_dim = key_cache.shape[-1]
    row_count = seq_count * prop_count
    tokens_wide = tokens.astype(jnp.float32)
    squares = lax.psum(jnp.sum(tokens_wide * tokens_wide, axis=-1), "kv")
    row_scale = lax.rsqrt(squares.reshape(row_count) / D + 1e-06)
    normed = (
        (tokens_wide * in_gain.astype(jnp.float32))
        .astype(jnp.bfloat16)
        .reshape(row_count, width_part)
    )
    starts = cache_len + accepted
    visible, depths = visible_links(parents)
    positions = (starts[:, None] + depths).reshape(row_count)
    part_q = jnp.dot(normed, query_weight, preferred_element_type=jnp.float32)
    part_k = jnp.dot(normed, key_weight, preferred_element_type=jnp.float32)
    part_v = jnp.dot(normed, value_weight, preferred_element_type=jnp.float32)
    sum_q, sum_k, sum_v = lax.psum((part_q, part_k, part_v), "kv")
    vec_shape = (sum_q.shape[0], heads_here, 2, head_dim)
    out_q = rotate((sum_q * row_scale[:, None]).reshape(vec_shape), positions).astype(jnp.bfloat16)
    out_k = rotate((sum_k * row_scale[:, None]).reshape(vec_shape), positions).astype(jnp.bfloat16)
    out_v = (sum_v * row_scale[:, None]).astype(jnp.bfloat16)
    query_blocks = out_q.reshape(seq_count, prop_count, heads_here, 2, head_dim)
    key_blocks = out_k.reshape(seq_count, prop_count, heads_here, 2, head_dim)
    value_blocks = out_v.reshape(seq_count, prop_count, heads_here, 2 * head_dim)
    offset = lax.axis_index("kv") * span_here
    slot_index = starts[:, None] + jnp.arange(prop_count, dtype=jnp.int32)[None, :] - offset
    slot_index = jnp.where((slot_index >= 0) & (slot_index < span_here), slot_index, span_here)
    seq_index = jnp.broadcast_to(jnp.arange(seq_count, dtype=jnp.int32)[:, None], slot_index.shape)
    key_out = key_cache.at[seq_index, slot_index].set(key_blocks, mode="drop")
    value_out = value_cache.at[seq_index, slot_index].set(value_blocks, mode="drop")
    inverse_root = head_dim ** (-0.5)
    cache_scores = (
        jnp.einsum(
            "bqhmd,bthmd->bhmqt", query_blocks, key_cache, preferred_element_type=jnp.float32
        )
        * inverse_root
    )
    live_mask = (offset + jnp.arange(span_here, dtype=jnp.int32))[None, :] < starts[:, None]
    live_mask = live_mask[:, None, None, None, :]
    cache_scores = jnp.where(live_mask, cache_scores, NEG_FILL)
    local_peak = jnp.max(cache_scores, axis=-1)
    local_total = jnp.sum(
        jnp.where(live_mask, jnp.exp(cache_scores - local_peak[..., None]), 0.0), axis=-1
    )
    cache_peak, cache_total = joined((local_peak, local_total), "kv", merge_stats)
    own_scores = (
        jnp.einsum(
            "bqhmd,bjhmd->bhmqj", query_blocks, key_blocks, preferred_element_type=jnp.float32
        )
        * inverse_root
    )
    seen_mask = visible[:, None, None]
    own_scores = jnp.where(seen_mask, own_scores, NEG_FILL)
    own_peak = jnp.max(own_scores, axis=-1)
    own_total = jnp.sum(
        jnp.where(seen_mask, jnp.exp(own_scores - own_peak[..., None]), 0.0), axis=-1
    )
    peak_all, totals = merge_stats((cache_peak, cache_total), (own_peak, own_total))
    lam_mix = lambdas[None, :, None, None]

    def weights_of(scores, alive):
        probs = jnp.where(alive, jnp.exp(scores - peak_all[..., None]), 0.0) / totals[..., None]
        return (probs[:, :, 0] - lam_mix * probs[:, :, 1]).astype(jnp.bfloat16)

    cache_weight = weights_of(cache_scores, live_mask)
    partial_value = jnp.einsum(
        "bhqt,bthe->bqhe", cache_weight, value_cache, preferred_element_type=jnp.float32
    )
    summed = lax.psum(partial_value.astype(jnp.bfloat16), "kv").astype(jnp.float32)
    own_weight = weights_of(own_scores, seen_mask)
    attended = summed + jnp.einsum(
        "bhqj,bjhe->bqhe", own_weight, value_blocks, preferred_element_type=jnp.float32
    )
    mixed_out = attended * lax.rsqrt(jnp.mean(attended * attended, axis=-1, keepdims=True) + 1e-05)
    mixed_out = (mixed_out * sub_gain.astype(jnp.float32) * LAMBDA_SCALE).astype(jnp.bfloat16)
    mixed_out = mixed_out.reshape(row_count, heads_here * 2 * head_dim)
    product = jnp.dot(mixed_out, out_weight, preferred_element_type=jnp.float32).reshape(
        seq_count, prop_count, -1
    )
    output = lax.psum_scatter(product.astype(jnp.bfloat16), "tp", scatter_dimension=2, tiled=True)
    return (output, key_out, value_out)


def solution(mesh):
    placed = (
        P("dp", None, "kv"),
        P("kv"),
        P("kv", "tp"),
        P("kv", "tp"),
        P("kv", "tp"),
        P("tp", "kv"),
        P("tp"),
        P(),
        P("dp", "kv", "tp", None, None),
        P("dp", "kv", "tp", None),
        P("dp"),
        P("dp"),
        P("dp", None),
    )
    return jax.shard_map(
        per_device,
        mesh=mesh,
        in_specs=placed,
        out_specs=(
            P("dp", None, ("kv", "tp")),
            P("dp", "kv", "tp", None, None),
            P("dp", "kv", "tp", None),
        ),
        check_vma=False,
    )
```

profile of v0, /device:TPU:26, one launch (start us, length us, event | category | flops | bytes accessed | tf_op | source)
XLA Modules:
  0.0 495.2 jit_solution(10723285334638067335)
XLA Ops:
  7.2 4.6 copy.162
  11.8 1.3 copy.163
  13.3 2.1 fusion.56
  15.4 2.1 fusion.57
  17.5 2.0 fusion.58
  19.6 18.3 %psum.36 = f32[16,16]{1,0:T(8,128)S(1)} all-reduce(f32[16,16]{1,0:T(8,128)S(1)} %get-tuple-element.111), channel_id=1, replica_groups=mesh['dp'=2,'kv'=8,'tp'=2] {'kv'}, use_global_device_ids=true, to_apply=%region_2.0 | all-reduce | flops 256 | bytes 2048 | tf_op jit(solution)/shard_map/psum | solution.py:85
  38.1 5.8 %while.24 = (s32[]{:T(128)}, f32[16,16,16]{2,1,0:T(8,128)S(1)}, s32[16,16]{1,0:T(8,128)S(1)}, s32[]{:T(128)}) while((s32[]{:T(128)}, f32[16,16,16]{2,1,0:T(8,128)S(1)}, s32[16,16]{1,0:T(8,128)S(1)}, s32[]{:T(128)}) %tuple.78), condition=%wide.region_4.0_spmd.clone, body=%wide.region_3.0_spmd.clone.sunk | while | flops 799234 | bytes 68661 | solution.py:36
  45.0 184.6 %all-reduce.6.cloned.1.call-done = (f32[256,2048]{1,0:T(8,128)}, f32[256,2048]{1,0:T(8,128)}, f32[256,2048]{1,0:T(8,128)}) async-done(((f32[256,2048]{1,0:T(8,128)}, f32[256,2048]{1,0:T(8,128)}, f32[256,2048]{1,0:T(8,128)}), (f32[256,2048]{1,0:T(8,128)}, f32[256,2048]{1,0:T(8,128)}, f32[256,2048]{1,0:T(8,128)})) %all-reduce.6.cloned.1.call-update) | async-done | bytes 6291472 | tf_op jit(solution)/shard_map/psum | solution.py:98
  229.6 5.5 %multiply_convert_fusion.1 = (bf16[256,2048]{1,0:T(8,128)(2,1)}, f32[256,2048]{1,0:T(8,128)}, f32[256,2048]{1,0:T(8,128)}) fusion(f32[256,2048]{1,0:T(8,128)} %get-tuple-element.94, f32[256]{0:T(256)S(1)} %rsqrt.19, f32[256,2048]{1,0:T(8,128)} %get-tuple-element.93, f32[256,2048]{1,0:T(8,128)} %get-tuple-element.92), kind=kLoop, calls=%fused_computation.27 | loop fusion | flops 2097152 | bytes 11535360 | tf_op jit(solution)/shard_map/convert_element_type | solution.py:102
  235.1 3.0 reshape.229
  238.2 4.0 reshape.230
  242.2 7.9 %fusion.52 = (f32[256,8,2,64]{3,2,1,0:T(2,128)S(1)}, f32[256,8,2,64]{3,2,1,0:T(2,128)S(1)}, f32[256,8,2,64]{3,2,1,0:T(2,128)S(1)}, f32[256,8,2,64]{3,2,1,0:T(2,128)S(1)}) fusion(f32[256,8,2,128]{3,2,1,0:T(2,128)} %reshape.230, f32[256,8,2,128]{3,2,1,0:T(2,128)S(1)} %reshape.229), kind=kLoop, calls=%fused_computation.89 | loop fusion | bytes 8388608 | tf_op jit(solution)/shard_map/slice | solution.py:47
  250.1 2.1 subtract_convert_fusion
  252.8 1.4 copy-done.5
  254.2 1.7 fusion.55
  255.9 1.4 select_reduce_fusion.1
  257.4 32.0 %all-gather.1 = f32[128,8,2,16]{3,1,2,0:T(8,128)S(1)} all-gather(f32[16,8,2,16]{3,1,2,0:T(8,128)S(1)} %copy.70), channel_id=3, replica_groups=mesh['dp'=2,'kv'=8,'tp'=2] {'kv'}, dimensions={0}, use_global_device_ids=true | all-gather | bytes 147456 | tf_op jit(solution)/shard_map/all_gather | solution.py:16
  290.4 32.6 %all-gather = f32[128,8,2,16]{3,1,2,0:T(8,128)S(1)} all-gather(f32[16,8,2,16]{3,1,2,0:T(8,128)S(1)} %copy.69), channel_id=2, replica_groups=mesh['dp'=2,'kv'=8,'tp'=2] {'kv'}, dimensions={0}, use_global_device_ids=true | all-gather | bytes 147456 | tf_op jit(solution)/shard_map/all_gather | solution.py:16
  324.2 9.0 %while.23 = (s32[]{:T(128)}, f32[16,8,2,16]{3,2,1,0:T(2,128)S(1)}, f32[16,8,2,16]{3,2,1,0:T(2,128)S(1)}, f32[7,16,8,2,16]{4,2,3,1,0:T(8,128)}, f32[7,16,8,2,16]{4,2,3,1,0:T(8,128)}, /*index=5*/s32[]{:T(128)}) while((s32[]{:T(128)}, f32[16,8,2,16]{3,2,1,0:T(2,128)S(1)}, f32[16,8,2,16]{3,2,1,0:T(2,128)S(1)}, f32[7,16,8,2,16]{4,2,3,1,0:T(8,128)}, ...), condition=%wide.region_9.10_spmd, body=%wide.region_8.9_spmd.sunk | while | flops 24578 | bytes 163913 | solution.py:19
  333.2 1.5 copy.78
  336.6 1.3 fusion.54
  339.4 1.5 select_divide_fusion.1
  341.0 1.6 fusion.21
  342.7 2.6 copy.98
  345.4 1.9 select_divide_fusion
  347.3 75.2 %all-reduce.4.cloned.1.call-done = bf16[16,16,8,256]{3,1,2,0:T(8,128)(2,1)} async-done(((bf16[16,16,8,256]{3,1,2,0:T(8,128)(2,1)}), bf16[16,16,8,256]{3,1,2,0:T(8,128)(2,1)}) %all-reduce.4.cloned.1.call-update) | async-done | bytes 1048592 | tf_op jit(solution)/shard_map/psum | solution.py:150
  422.4 2.9 multiply_reduce_fusion
  425.9 1.1 copy-done.22
  427.0 1.4 fusion.24
  429.1 2.1 copy.87
  431.1 32.4 %scatter_fusion = bf16[16,32,8,2,128]{4,3,2,1,0:T(2,128)(2,1)} fusion(bf16[16,32,8,2,128]{4,3,2,1,0:T(2,128)(2,1)} %copy.162, s32[256]{0:T(256)S(1)} %reshape.232, bf16[256,8,2,128]{3,2,1,0:T(2,128)(2,1)} %copy.87), kind=kCustom, calls=%fused_computation | custom fusion | bytes 3147776 | tf_op jit(solution)/shard_map/scatter | solution.py:110
  463.5 25.1 %scatter_fusion.1 = bf16[16,32,8,256]{3,2,1,0:T(8,128)(2,1)} fusion(bf16[16,32,8,256]{3,2,1,0:T(8,128)(2,1)} %copy.163, s32[256]{0:T(256)S(1)} %reshape.232, bf16[256,8,256]{2,1,0:T(8,128)(2,1)S(1)} %bitcast.96), kind=kCustom, calls=%fused_computation.1 | custom fusion | bytes 3147776 | tf_op jit(solution)/shard_map/scatter | solution.py:111
  (156 shorter events, 23.0 us)
Async XLA Ops:
  7.2 6.2 %copy-start = (bf16[512,2048]{1,0:T(8,128)(2,1)S(1)}, bf16[512,2048]{1,0:T(8,128)(2,1)}, u32[]{:S(2)}) copy-start(bf16[512,2048]{1,0:T(8,128)(2,1)} %param.19) | copy-start | bytes 6291460
  7.2 222.4 %all-reduce.6.cloned.1.call-start = ((), (), s32[]{:S(2)}) async-start(), calls=%async_computation.3 | async-start | bytes 12582912 | tf_op jit(solution)/shard_map/psum | solution.py:98
  7.2 4.6 copy-start.11
  11.8 1.3 copy-start.21
  11.8 1.3 copy-start.18
  13.3 2.1 copy-start.12
  15.4 2.1 copy-start.13
  19.5 18.5 %copy-start.19 = (s32[16,16]{1,0:T(8,128)S(1)}, s32[16,16]{1,0:T(8,128)}, u32[]{:S(2)}) copy-start(s32[16,16]{1,0:T(8,128)} %param.29) | copy-start | bytes 3076
  19.6 24.4 %copy-start.23 = (s32[16]{0:T(128)S(1)}, s32[16]{0:T(128)}, u32[]{:S(2)}) copy-start(s32[16]{0:T(128)} %param.27) | copy-start | bytes 196
  19.6 24.4 %copy-start.24 = (s32[16]{0:T(128)S(1)}, s32[16]{0:T(128)}, u32[]{:S(2)}) copy-start(s32[16]{0:T(128)} %param.28) | copy-start | bytes 196
  19.6 402.8 %all-reduce.4.cloned.1.call-start = ((), (), s32[]{:S(2)}) async-start(), calls=%async_computation.1 | async-start | bytes 2097152 | tf_op jit(solution)/shard_map/psum | solution.py:150
  44.3 293.6 %copy-start.16 = (pred[16,16,16]{1,2,0:T(8,128)(4,1)}, pred[16,16,16]{1,2,0:T(8,128)(4,1)S(1)}, u32[]{:S(2)}) copy-start(pred[16,16,16]{1,2,0:T(8,128)(4,1)S(1)} %copy.75) | copy-start | bytes 12292
  252.2 2.0 copy-start.5
  252.5 3.4 copy-start.7
  254.2 1.7 copy-start.9
  335.0 1.2 copy-start.8
  335.0 1.5 copy-start.10
  337.9 3.0 copy-start.2
  338.8 0.7 copy-start.14
  339.4 1.6 copy-start.4
  339.4 1.6 copy-start.20
  341.0 1.6 copy-start.25
  342.6 2.7 copy-start.3
  342.6 2.7 copy-start.15
  342.6 2.7 copy-start.17
  342.6 146.0 %reduce-scatter.2.cloned.1.call-start = ((), (), s32[]{:S(2)}) async-start(), calls=%async_computation.2 | async-start | bytes 393216 | tf_op jit(solution)/shard_map/reduce_scatter | solution.py:161
  425.4 1.6 copy-start.22
  431.1 32.4 %copy-start.6 = (bf16[32,8,8,256]{3,2,1,0:T(8,128)(2,1)S(1)}, bf16[32,8,8,256]{3,2,1,0:T(8,128)(2,1)}, u32[]{:S(2)}) copy-start(bf16[32,8,8,256]{3,2,1,0:T(8,128)(2,1)} %copy.98) | copy-start | bytes 3145732
  431.1 57.5 %copy-start.1 = (bf16[512,2048]{1,0:T(8,128)(2,1)S(1)}, bf16[512,2048]{1,0:T(8,128)(2,1)}, u32[]{:S(2)}) copy-start(bf16[512,2048]{1,0:T(8,128)(2,1)} %param.19) | copy-start | bytes 6291460
Sparse Core Ops, SparseCore 0:
  19.7 209.8 all-reduce.5
  342.8 79.6 all-reduce.3
  428.5 8.7 reduce-scatter.1
where the time goes:
time: 497 us; the launch traced here: 495 us
  waiting for transfers between devices  260 us (52%)
  local copies, waits for them, and re-layouts  99.9 us (20%)
  blocking collectives  83 us (17%)
  matrix products  20 us (4%)
  other arithmetic  17.5 us (4%)
  between operations  14.2 us (3%)
    psum x1, waiting for transfers between devices, per_device(): sum_q, sum_k, sum_v = lax.psum((part_q, part_k, part_v), 'kv')  185 us
    psum x1, waiting for transfers between devices, per_device(): lax.psum(partial_value.astype(jnp.bfloat16), 'kv').astype(jnp.float32)  75.2 us
    all_gather x2, blocking collectives, joined(): pieces = jax.tree.map(lambda part: lax.all_gather(part, axis), value)  64.7 us
    scatter x1, local copies, waits for them, and re-layouts, per_device(): key_out = key_cache.at[seq_index, slot_index].set(key_blocks, mode='drop')  32.4 us
    scatter x1, local copies, waits for them, and re-layouts, per_device(): value_cache.at[seq_index, slot_index].set(value_blocks, mode='drop')  25.1 us
    psum x1, blocking collectives, per_device(): squares = lax.psum(jnp.sum(tokens_wide * tokens_wide, axis=-1), 'kv')  18.3 us
    unnamed x55, local copies, waits for them, and re-layouts  12.8 us
  transfers between devices with their start and end apart: 3, of which 2 were waited for; matrix products, arithmetic and copies ran while one was open for 14% of the time, Pallas kernels for 0%

commit v1 on v0

v1 whole, which is shorter than its diff:
```python
import math

import jax
import jax.numpy as jnp
from jax import lax
from jax.sharding import PartitionSpec as P

LAMBDA_SCALE = 0.2 + 0.6 * math.exp(-0.6)
NEG_FILL = -1e30
F32 = jnp.float32
BF16 = jnp.bfloat16


def grid_of(kv):
    inner = 1
    while kv % (inner * 2) == 0 and (inner * 2) ** 2 <= kv:
        inner *= 2
    return kv // inner, inner


def visible_links(parents):
    number = parents.shape[-1]
    identity = jnp.eye(number, dtype=F32)
    links = (parents[..., :, None] == jnp.arange(number, dtype=jnp.int32)).astype(F32)
    reached = jnp.maximum(links, identity)
    span = 1
    while span < number:
        reached = jnp.minimum(
            jnp.einsum("bij,bjk->bik", reached.astype(BF16), reached.astype(BF16), preferred_element_type=F32), 1.0
        )
        span *= 2
    depths = (jnp.sum(reached, axis=-1) - 1.0).astype(jnp.int32)
    return reached > 0.5, depths


def turn_table(positions, half_dim):
    frequency = 10000.0 ** (-jnp.arange(half_dim, dtype=F32) / half_dim)
    angles = positions.astype(F32)[..., None] * frequency
    return jnp.cos(angles), jnp.sin(angles)


def rotate(values, table):
    cosine, sine = (part[:, None, None, :] for part in table)
    half_dim = values.shape[-1] // 2
    low = values[..., :half_dim]
    high = values[..., half_dim:]
    return jnp.concatenate([low * cosine - high * sine, high * cosine + low * sine], axis=-1)


def merge_stats(former, latter):
    highest = jnp.maximum(former[0], latter[0])
    totals = former[1] * jnp.exp(former[0] - highest) + latter[1] * jnp.exp(latter[0] - highest)
    return (highest, totals)


def make_body(kv, tp):
    Z, Y = grid_of(kv)

    def body(
        tokens, in_gain, query_weight, key_weight, value_weight, out_weight, lambdas, sub_gain,
        key_cache, value_cache, cache_len, accepted, parents,
    ):
        seqs, props, width = tokens.shape
        heads = lambdas.shape[0]
        span = key_cache.shape[1]
        hd = key_cache.shape[-1]
        Sy = seqs // Y
        Ry = Sy * props
        Hz = heads // Z
        cz = Hz * 2 * hd
        width_all = width * kv
        k = lax.axis_index("kv")
        y = k % Y
        z = k // Y

        def yperm(x, s):
            return lax.ppermute(x, "kv", [(i, (i // Y) * Y + ((i % Y) ^ s)) for i in range(kv)])

        def zperm(x, s):
            return lax.ppermute(x, "kv", [(i, ((i // Y) ^ s) * Y + i % Y) for i in range(kv)])

        def natural(parts, index):
            parts = list(parts)
            bit = 1
            while bit < len(parts):
                odd = (index & bit) != 0
                parts = [jnp.where(odd, parts[s ^ bit], parts[s]) for s in range(len(parts))]
                bit *= 2
            return parts

        def yrows(a, which):
            size = a.shape[0] // Y
            return lax.dynamic_slice_in_dim(a, which * size, size, 0)

        def zcols(a, which):
            return lax.dynamic_slice_in_dim(a, which * cz, cz, 1)

        wide = tokens.astype(F32)
        normed = (wide * in_gain.astype(F32)).astype(BF16).reshape(seqs * props, width)
        squares = jnp.sum(wide * wide, axis=-1).reshape(seqs * props)

        def send_y(weight):
            return [
                yperm(jnp.dot(yrows(normed, y ^ s), weight, preferred_element_type=F32).astype(BF16), s)
                for s in range(1, Y)
            ]

        def sum_y(weight, got):
            total = jnp.dot(yrows(normed, y), weight, preferred_element_type=F32)
            for part in got:
                total = total + part.astype(F32)
            return total

        def send_z(total):
            return [zperm(zcols(total, z ^ s).astype(BF16), s) for s in range(1, Z)]

        def sum_z(total, got):
            total = zcols(total, z)
            for part in got:
                total = total + part.astype(F32)
            return total

        got_q = send_y(query_weight)
        sq = yrows(squares, y)
        for part in [yperm(yrows(squares, y ^ s), s) for s in range(1, Y)]:
            sq = sq + part
        for part in [zperm(sq, s) for s in range(1, Z)]:
            sq = sq + part
        row_scale = lax.rsqrt(sq / width_all + 1e-06)[:, None]

        sum_q = sum_y(query_weight, got_q)
        got_qz = send_z(sum_q)
        got_k = send_y(key_weight)
        sum_k = sum_y(key_weight, got_k)
        got_kz = send_z(sum_k)
        got_v = send_y(value_weight)
        sum_v = sum_y(value_weight, got_v)
        got_vz = send_z(sum_v)

        starts_all = cache_len + accepted
        starts = yrows(starts_all, y)
        visible, depths = visible_links(yrows(parents, y))
        table = turn_table((starts[:, None] + depths).reshape(Ry), hd // 2)

        vec = (Ry, Hz, 2, hd)
        q_own = rotate((sum_z(sum_q, got_qz) * row_scale).reshape(vec), table).astype(BF16).reshape(Ry, cz)
        q_all = natural([q_own] + [zperm(q_own, s) for s in range(1, Z)], z)
        q_all = jnp.stack(q_all).reshape(Z, Sy, props, Hz, 2, hd)
        k_own = rotate((sum_z(sum_k, got_kz) * row_scale).reshape(vec), table).astype(BF16).reshape(Ry, cz)
        v_own = (sum_z(sum_v, got_vz) * row_scale).astype(BF16)

        def cache_y(cache):
            parts = [yrows(cache, y)] + [yperm(yrows(cache, y ^ s), s) for s in range(1, Y)]
            return jnp.stack(parts, axis=1)

        keys = cache_y(key_cache).reshape(Sy, Y * span, Z, Hz, 2, hd)
        values = cache_y(value_cache).reshape(Sy, Y * span, Z, Hz, 2 * hd)
        order = jnp.stack([z * Y + (y ^ s) for s in range(Y)])
        spots = (order[:, None] * span + jnp.arange(span, dtype=jnp.int32)).reshape(Y * span)
        live = (spots[None, :] < starts[:, None])[None, :, None, None, None, :]

        inverse_root = hd ** (-0.5)
        scores = (
            jnp.einsum("zbqhmd,btzhmd->zbhmqt", q_all, keys, preferred_element_type=F32) * inverse_root
        )
        scores = jnp.where(live, scores, NEG_FILL)
        local_peak = jnp.max(scores, axis=-1)
        local_total = jnp.sum(jnp.where(live, jnp.exp(scores - local_peak[..., None]), 0.0), axis=-1)

        q_b = q_own.reshape(Sy, props, Hz, 2, hd)
        k_b = k_own.reshape(Sy, props, Hz, 2, hd)
        v_b = v_own.reshape(Sy, props, Hz, 2 * hd)
        own_scores = jnp.einsum("bqhmd,bjhmd->bhmqj", q_b, k_b, preferred_element_type=F32) * inverse_root
        seen = visible[:, None, None]
        own_scores = jnp.where(seen, own_scores, NEG_FILL)
        own_peak = jnp.max(own_scores, axis=-1)
        own_total = jnp.sum(jnp.where(seen, jnp.exp(own_scores - own_peak[..., None]), 0.0), axis=-1)

        mine = jnp.stack([local_peak, local_total])
        own_stats = jnp.stack([own_peak, own_total])
        packed = jnp.concatenate([mine, own_stats[:, None]], axis=1)
        got = [packed] + [zperm(packed, s) for s in range(1, Z)]
        stat = (mine[0], mine[1])
        for part in got[1:]:
            stat = merge_stats(stat, (part[0, :Z], part[1, :Z]))
        own_all = jnp.stack(natural([part[:, Z] for part in got], z))
        peak_all, totals = merge_stats(stat, (own_all[:, 0], own_all[:, 1]))

        def at_z(a, which):
            return lax.dynamic_index_in_dim(a, which, 0, keepdims=False)

        lam = lambdas.reshape(Z, Hz)

        def weights_of(scores, alive, peak, total, lam_mix):
            probs = jnp.where(alive, jnp.exp(scores - peak[..., None]), 0.0) / total[..., None]
            return (probs[..., 0, :, :] - lam_mix * probs[..., 1, :, :]).astype(BF16)

        cache_weight = weights_of(scores, live, peak_all, totals, lam[:, None, :, None, None])
        partial = jnp.einsum("zbhqt,btzhe->zbqhe", cache_weight, values, preferred_element_type=F32)
        attended = at_z(partial, z).astype(BF16).astype(F32)
        for part in [zperm(at_z(partial, z ^ s).astype(BF16), s) for s in range(1, Z)]:
            attended = attended + part.astype(F32)
        own_weight = weights_of(
            own_scores, seen, at_z(peak_all, z), at_z(totals, z), at_z(lam, z)[None, :, None, None]
        )
        attended = attended + jnp.einsum("bhqj,bjhe->bqhe", own_weight, v_b, preferred_element_type=F32)
        mixed = attended * lax.rsqrt(jnp.mean(attended * attended, axis=-1, keepdims=True) + 1e-05)
        mixed = (mixed * sub_gain.astype(F32) * LAMBDA_SCALE).astype(BF16).reshape(Ry, cz)

        def spread(chunk):
            whole = jnp.concatenate(natural([chunk] + [zperm(chunk, s) for s in range(1, Z)], z), axis=-1)
            return [whole] + [yperm(whole, s) for s in range(1, Y)]

        products = [
            jnp.dot(rows, out_weight, preferred_element_type=F32).astype(BF16) for rows in spread(mixed)
        ]
        product = jnp.concatenate(natural(products, y), axis=0).reshape(seqs, props, -1)
        share = product.shape[-1] // tp
        t = lax.axis_index("tp")

        def tcols(which):
            return lax.dynamic_slice_in_dim(product, which * share, share, 2)

        output = tcols(t).astype(F32)
        for s in range(1, tp):
            output = output + lax.ppermute(
                tcols(t ^ s), "tp", [(i, i ^ s) for i in range(tp)]
            ).astype(F32)
        output = output.astype(BF16)

        kv_new = jnp.stack([k_own, v_own])
        new_all = jnp.concatenate(natural(spread(kv_new), y), axis=1)
        offset = k * span
        slot = offset + jnp.arange(span, dtype=jnp.int32)[None, :] - starts_all[:, None]
        pick = (slot[:, :, None] == jnp.arange(props, dtype=jnp.int32)).astype(BF16)
        fresh = (slot >= 0) & (slot < props)
        new_all = new_all.reshape(2, seqs, props, heads * 2 * hd)

        def written(cache, new):
            moved = jnp.einsum("btj,bje->bte", pick, new, preferred_element_type=F32).astype(BF16)
            flat = moved.reshape(cache.shape)
            mask = fresh.reshape(fresh.shape + (1,) * (cache.ndim - 2))
            return jnp.where(mask, flat, cache)

        return (output, written(key_cache, new_all[0]), written(value_cache, new_all[1]))

    return body


def solution(mesh):
    placed = (
        P("dp", None, "kv"),
        P("kv"),
        P("kv", "tp"),
        P("kv", "tp"),
        P("kv", "tp"),
        P("tp", "kv"),
        P("tp"),
        P(),
        P("dp", "kv", "tp", None, None),
        P("dp", "kv", "tp", None),
        P("dp"),
        P("dp"),
        P("dp", None),
    )
    return jax.shard_map(
        make_body(mesh.shape["kv"], mesh.shape["tp"]),
        mesh=mesh,
        in_specs=placed,
        out_specs=(
            P("dp", None, ("kv", "tp")),
            P("dp", "kv", "tp", None, None),
            P("dp", "kv", "tp", None),
        ),
        check_vma=False,
    )
```

time: 497 us -> 198 us (0.40)
  waiting for transfers between devices: 260 us -> 81 us
  blocking collectives: 83 us -> 0 us
  local copies, waits for them, and re-layouts: 99.9 us -> 18.8 us
  starting transfers between devices: 0.12 us -> 50 us
  between operations: 14.2 us -> 1.5 us
  other arithmetic: 17.5 us -> 26 us
    psum x2 -> x0, waiting for transfers between devices: 260 us -> none  [the longest x1 185 us: per_device(): sum_q, sum_k, sum_v = lax.psum((part_q, part_k, part_v), 'kv')]
    ppermute x0 -> x36, waiting for transfers between devices: none -> 81 us  [the longest x27 54.3 us: zperm(): lax.ppermute(x, 'kv', [(i, (i // Y ^ s) * Y + i % Y) for i in range(kv)])]
    all_gather x2 -> x0, blocking collectives: 64.7 us -> none  [joined(): pieces = jax.tree.map(lambda part: lax.all_gather(part, axis), value)]
    scatter x2 -> x0, local copies, waits for them, and re-layouts: 57.5 us -> none  [the longest x1 32.4 us: per_device(): key_out = key_cache.at[seq_index, slot_index].set(key_blocks, mode='drop')]
    ppermute x0 -> x36, starting transfers between devices: none -> 50 us  [the longest x27 40.2 us: zperm(): lax.ppermute(x, 'kv', [(i, (i // Y ^ s) * Y + i % Y) for i in range(kv)])]
    psum x1 -> x0, blocking collectives: 18.3 us -> none  [per_device(): squares = lax.psum(jnp.sum(tokens_wide * tokens_wide, axis=-1), 'kv')]
    select_n x0 -> x8, other arithmetic: none -> 10.1 us  [the longest x2 5.37 us: written(): return jnp.where(mask, flat, cache)]
    slice x5 -> x0, local copies, waits for them, and re-layouts: 9.91 us -> none  [the longest x1 7.9 us: rotate(): lower_half = values[..., :half_dim]]
  transfers between devices with their start and end apart: 3 -> 36, of which waited for: 2 -> 15; matrix products, arithmetic and copies ran while one was open for 14% -> 27% of each run, Pallas kernels for 0% -> 0%
where the time goes in v1:
time: 198 us; the launch traced here: 195 us
  waiting for transfers between devices  81 us (41%)
  starting transfers between devices  50 us (25%)
  other arithmetic  26 us (13%)
  local copies, waits for them, and re-layouts  18.8 us (9%)
  matrix products  17.5 us (9%)
    ppermute x27, waiting for transfers between devices, zperm(): lax.ppermute(x, 'kv', [(i, (i // Y ^ s) * Y + i % Y) for i in range(kv)])  54.3 us
    ppermute x27, starting transfers between devices, zperm(): lax.ppermute(x, 'kv', [(i, (i // Y ^ s) * Y + i % Y) for i in range(kv)])  40.2 us
    ppermute x8, waiting for transfers between devices, yperm(): lax.ppermute(x, 'kv', [(i, i // Y * Y + (i % Y ^ s)) for i in range(kv)])  26.7 us
    ppermute x8, starting transfers between devices, yperm(): lax.ppermute(x, 'kv', [(i, i // Y * Y + (i % Y ^ s)) for i in range(kv)])  9.89 us
    dynamic_slice x7, local copies, waits for them, and re-layouts, yrows(): return lax.dynamic_slice_in_dim(a, which * size, size, 0)  6.42 us
    unnamed x72, local copies, waits for them, and re-layouts  5.98 us
    dot_general x3, matrix products, send_y(): jnp.dot(yrows(normed, y ^ s), weight, preferred_element_type=F32)  5.41 us
    select_n x2, other arithmetic, written(): return jnp.where(mask, flat, cache)  5.37 us
  transfers between devices with their start and end apart: 36, of which 15 were waited for; matrix products, arithmetic and copies ran while one was open for 27% of the time, Pallas kernels for 0%

profile of v1, /device:TPU:26, one launch (start us, length us, event | category | flops | bytes accessed | tf_op | source)
XLA Modules:
  0.0 194.8 jit_solution(9236525815223349410)
XLA Ops:
  6.1 2.9 %convolution_convert_fusion.3 = bf16[128,2048]{1,0:T(8,128)(2,1)} fusion(bf16[512,2048]{1,0:T(8,128)(2,1)} %param.16, bf16[256,512]{1,0:T(8,128)(2,1)S(1)} %bitcast.252, s32[]{:T(128)S(6)} %select_n.361), kind=kOutput, calls=%fused_computation.4 | convolution fusion | flops 268697600 | bytes 2752516 | tf_op jit(solution)/shard_map/dot_general | solution.py:104
  13.9 3.1 %constant_dynamic-slice_fusion.3 = (bf16[8,32,8,2,128]{4,3,2,1,0:T(2,128)(2,1)S(1)}, bf16[8,32,8,2,128]{4,3,2,1,0:T(2,128)(2,1)S(1)}) fusion(bf16[16,32,8,2,128]{4,3,2,1,0:T(2,128)(2,1)} %param.21, s32[]{:T(128)S(6)} %select_n.358, s32[]{:T(128)S(6)} %select_n.359), kind=kLoop, calls=%fused_computation.203 | loop fusion | bytes 4194312 | tf_op jit(solution)/shard_map/dynamic_slice | solution.py:93
  25.9 1.7 collective-permute-start.7
  29.1 2.0 %collective-permute-start.26 = (bf16[128,512]{1,0:T(8,128)(2,1)S(1)}, bf16[128,512]{1,0:T(8,128)(2,1)S(1)}, u32[]{:S(2)}, u32[]{:S(2)}) collective-permute-start(bf16[128,512]{1,0:T(8,128)(2,1)S(1)} %get-tuple-element.18), channel_id=1, source_target_pairs={{0,12},{2,14},{4,8},{6,10},{8,4},{10,6},{12,0},{14,2},{1,13},{3,15... | collective-permute-start | bytes 393224 | tf_op jit(solution)/shard_map/ppermute | solution.py:80
  31.1 2.0 %collective-permute-start.25 = (bf16[128,512]{1,0:T(8,128)(2,1)S(1)}, bf16[128,512]{1,0:T(8,128)(2,1)S(1)}, u32[]{:S(2)}, u32[]{:S(2)}) collective-permute-start(bf16[128,512]{1,0:T(8,128)(2,1)S(1)} %get-tuple-element.19), channel_id=1, source_target_pairs={{0,8},{2,10},{4,12},{6,14},{8,0},{10,2},{12,4},{14,6},{1,9},{3,11}... | collective-permute-start | bytes 393224 | tf_op jit(solution)/shard_map/ppermute | solution.py:80
  35.2 5.1 %collective-permute-done.1 = bf16[128,2048]{1,0:T(8,128)(2,1)} collective-permute-done((bf16[128,2048]{1,0:T(8,128)(2,1)}, bf16[128,2048]{1,0:T(8,128)(2,1)}, u32[]{:S(2)}, u32[]{:S(2)}) %collective-permute-start.1) | collective-permute-done | bytes 524320 | tf_op jit(solution)/shard_map/ppermute | solution.py:77
  42.9 2.8 %collective-permute-done.6 = f32[128]{0:T(128)S(1)} collective-permute-done((f32[128]{0:T(128)S(1)}, f32[128]{0:T(128)S(1)}, u32[]{:S(2)}, u32[]{:S(2)}) %collective-permute-start.6) | collective-permute-done | bytes 544 | tf_op jit(solution)/shard_map/ppermute | solution.py:80
  45.7 2.1 %collective-permute-start.15 = (bf16[128,512]{1,0:T(8,128)(2,1)S(1)}, bf16[128,512]{1,0:T(8,128)(2,1)S(1)}, u32[]{:S(2)}, u32[]{:S(2)}) collective-permute-start(bf16[128,512]{1,0:T(8,128)(2,1)S(1)} %get-tuple-element.22), channel_id=1, source_target_pairs={{0,8},{2,10},{4,12},{6,14},{8,0},{10,2},{12,4},{14,6},{1,9},{3,11}... | collective-permute-start | bytes 393224 | tf_op jit(solution)/shard_map/ppermute | solution.py:80
  47.8 2.0 %collective-permute-start.14 = (bf16[128,512]{1,0:T(8,128)(2,1)S(1)}, bf16[128,512]{1,0:T(8,128)(2,1)S(1)}, u32[]{:S(2)}, u32[]{:S(2)}) collective-permute-start(bf16[128,512]{1,0:T(8,128)(2,1)S(1)} %get-tuple-element.20), channel_id=1, source_target_pairs={{0,4},{2,6},{4,0},{6,2},{8,12},{10,14},{12,8},{14,10},{1,5},{3,7},... | collective-permute-start | bytes 393224 | tf_op jit(solution)/shard_map/ppermute | solution.py:80
  51.4 2.9 %collective-permute-start.2 = (bf16[128,512]{1,0:T(8,128)(2,1)S(1)}, bf16[128,512]{1,0:T(8,128)(2,1)S(1)}, u32[]{:S(2)}, u32[]{:S(2)}) collective-permute-start(bf16[128,512]{1,0:T(8,128)(2,1)S(1)} %get-tuple-element.23), channel_id=1, source_target_pairs={{0,4},{2,6},{4,0},{6,2},{8,12},{10,14},{12,8},{14,10},{1,5},{3,7},... | collective-permute-start | bytes 393224 | tf_op jit(solution)/shard_map/ppermute | solution.py:80
  54.3 5.6 %collective-permute-done.15 = bf16[128,512]{1,0:T(8,128)(2,1)S(1)} collective-permute-done((bf16[128,512]{1,0:T(8,128)(2,1)S(1)}, bf16[128,512]{1,0:T(8,128)(2,1)S(1)}, u32[]{:S(2)}, u32[]{:S(2)}) %collective-permute-start.15) | collective-permute-done | bytes 131104 | tf_op jit(solution)/shard_map/ppermute | solution.py:80
  61.4 4.2 %collective-permute-done.3 = bf16[128,512]{1,0:T(8,128)(2,1)S(1)} collective-permute-done((bf16[128,512]{1,0:T(8,128)(2,1)S(1)}, bf16[128,512]{1,0:T(8,128)(2,1)S(1)}, u32[]{:S(2)}, u32[]{:S(2)}) %collective-permute-start.3) | collective-permute-done | bytes 131104 | tf_op jit(solution)/shard_map/ppermute | solution.py:80
  67.9 3.1 %collective-permute-start.11 = (bf16[128,512]{0,1:T(8,128)(2,1)S(1)}, bf16[128,512]{0,1:T(8,128)(2,1)S(1)}, u32[]{:S(2)}, u32[]{:S(2)}) collective-permute-start(bf16[128,512]{0,1:T(8,128)(2,1)S(1)} %bitcast.272), channel_id=1, source_target_pairs={{0,4},{2,6},{4,0},{6,2},{8,12},{10,14},{12,8},{14,10},{1,5},{3,7},... | collective-permute-start | bytes 393224 | tf_op jit(solution)/shard_map/ppermute | solution.py:80
  74.7 4.9 %collective-permute-start.33 = (bf16[2,128,512]{2,1,0:T(8,128)(2,1)}, bf16[2,128,512]{2,1,0:T(8,128)(2,1)}, u32[]{:S(2)}, u32[]{:S(2)}) collective-permute-start(bf16[2,128,512]{2,1,0:T(8,128)(2,1)} %pad_maximum_fusion.6), channel_id=1, source_target_pairs={{0,8},{2,10},{4,12},{6,14},{8,0},{10,2},{12,4},{14,6},{1,9},{3,11}... | collective-permute-start | bytes 786440 | tf_op jit(solution)/shard_map/ppermute | solution.py:80
  79.6 10.0 %collective-permute-done.10 = bf16[128,512]{0,1:T(8,128)(2,1)S(1)} collective-permute-done((bf16[128,512]{0,1:T(8,128)(2,1)S(1)}, bf16[128,512]{0,1:T(8,128)(2,1)S(1)}, u32[]{:S(2)}, u32[]{:S(2)}) %collective-permute-start.10) | collective-permute-done | bytes 131104 | tf_op jit(solution)/shard_map/ppermute | solution.py:80
  92.9 7.8 %collective-permute-done.33 = bf16[2,128,512]{2,1,0:T(8,128)(2,1)} collective-permute-done((bf16[2,128,512]{2,1,0:T(8,128)(2,1)}, bf16[2,128,512]{2,1,0:T(8,128)(2,1)}, u32[]{:S(2)}, u32[]{:S(2)}) %collective-permute-start.33) | collective-permute-done | bytes 262176 | tf_op jit(solution)/shard_map/ppermute | solution.py:80
  102.0 2.1 %broadcast_select_fusion.10 = (bf16[2,128,512]{2,1,0:T(8,128)(2,1)S(1)}, bf16[2,128,512]{2,1,0:T(8,128)(2,1)}, bf16[2,128,512]{2,1,0:T(8,128)(2,1)}, bf16[2,128,512]{2,1,0:T(8,128)(2,1)}) fusion(pred[]{:T(512)S(6)} %ne.31, bf16[2,128,512]{2,1,0:T(8,128)(2,1)} %collective-permute-done.32, bf16[2,128,512]{2,1,0:T(8,128)(2,1)} %collective-permute-done.33, ...), kind=kLoop, calls=%fused_computation.93 | loop fusion | flops 1179648 | bytes 2097154 | tf_op jit(solution)/shard_map/jit(_where)/select_n | solution.py:87
  108.0 3.0 %collective-permute-start.19 = (f32[2,5,8,2,2,16]{5,4,3,2,1,0:T(2,128)S(1)}, f32[2,5,8,2,2,16]{5,4,3,2,1,0:T(2,128)S(1)}, u32[]{:S(2)}, u32[]{:S(2)}) collective-permute-start(f32[2,5,8,2,2,16]{5,4,3,2,1,0:T(2,128)S(1)} %pad_maximum_fusion.7), channel_id=1, source_target_pairs={{0,12},{2,14},{4,8},{6,10},{8,4},{10,6},{12,0},{14,2},{1,13},{3,15... | collective-permute-start | bytes 61448 | tf_op jit(solution)/shard_map/ppermute | solution.py:80
  114.0 3.0 %collective-permute-done.19 = f32[2,5,8,2,2,16]{5,4,3,2,1,0:T(2,128)S(1)} collective-permute-done((f32[2,5,8,2,2,16]{5,4,3,2,1,0:T(2,128)S(1)}, f32[2,5,8,2,2,16]{5,4,3,2,1,0:T(2,128)S(1)}, u32[]{:S(2)}, u32[]{:S(2)}) %collective-permute-start.19) | collective-permute-done | bytes 20512 | tf_op jit(solution)/shard_map/ppermute | solution.py:80
  116.9 5.7 %collective-permute-done.18 = f32[2,5,8,2,2,16]{5,4,3,2,0,1:T(2,128)S(1)} collective-permute-done((f32[2,5,8,2,2,16]{5,4,3,2,0,1:T(2,128)S(1)}, f32[2,5,8,2,2,16]{5,4,3,2,0,1:T(2,128)S(1)}, u32[]{:S(2)}, u32[]{:S(2)}) %collective-permute-start.18) | collective-permute-done | bytes 20512 | tf_op jit(solution)/shard_map/ppermute | solution.py:80
  124.5 2.2 %collective-permute-start.22 = (bf16[8,16,2,256]{3,1,2,0:T(8,128)(2,1)S(1)}, bf16[8,16,2,256]{3,1,2,0:T(8,128)(2,1)S(1)}, u32[]{:S(2)}, u32[]{:S(2)}) collective-permute-start(bf16[8,16,2,256]{3,1,2,0:T(8,128)(2,1)S(1)} %get-tuple-element.31), channel_id=1, source_target_pairs={{0,12},{2,14},{4,8},{6,10},{8,4},{10,6},{12,0},{14,2},{1,13},{3,15... | collective-permute-start | bytes 393224 | tf_op jit(solution)/shard_map/ppermute | solution.py:80
  126.7 2.3 %collective-permute-start.20 = (bf16[8,16,2,256]{3,1,2,0:T(8,128)(2,1)S(1)}, bf16[8,16,2,256]{3,1,2,0:T(8,128)(2,1)S(1)}, u32[]{:S(2)}, u32[]{:S(2)}) collective-permute-start(bf16[8,16,2,256]{3,1,2,0:T(8,128)(2,1)S(1)} %get-tuple-element.30), channel_id=1, source_target_pairs={{0,4},{2,6},{4,0},{6,2},{8,12},{10,14},{12,8},{14,10},{1,5},{3,7},... | collective-permute-start | bytes 393224 | tf_op jit(solution)/shard_map/ppermute | solution.py:80
  129.1 3.7 %collective-permute-done.22 = bf16[8,16,2,256]{3,1,2,0:T(8,128)(2,1)S(1)} collective-permute-done((bf16[8,16,2,256]{3,1,2,0:T(8,128)(2,1)S(1)}, bf16[8,16,2,256]{3,1,2,0:T(8,128)(2,1)S(1)}, u32[]{:S(2)}, u32[]{:S(2)}) %collective-permute-start.22) | collective-permute-done | bytes 131104 | tf_op jit(solution)/shard_map/ppermute | solution.py:80
  132.8 4.0 %collective-permute-done.21 = bf16[8,16,2,256]{3,1,2,0:T(8,128)(2,1)S(1)} collective-permute-done((bf16[8,16,2,256]{3,1,2,0:T(8,128)(2,1)S(1)}, bf16[8,16,2,256]{3,1,2,0:T(8,128)(2,1)S(1)}, u32[]{:S(2)}, u32[]{:S(2)}) %collective-permute-start.21) | collective-permute-done | bytes 131104 | tf_op jit(solution)/shard_map/ppermute | solution.py:80
  137.5 1.8 collective-permute-start.27
  139.3 2.7 %collective-permute-start.29 = (bf16[128,512]{0,1:T(8,128)(2,1)S(1)}, bf16[128,512]{0,1:T(8,128)(2,1)S(1)}, u32[]{:S(2)}, u32[]{:S(2)}) collective-permute-start(bf16[128,512]{0,1:T(8,128)(2,1)S(1)} %copy.98), channel_id=1, source_target_pairs={{0,4},{2,6},{4,0},{6,2},{8,12},{10,14},{12,8},{14,10},{1,5},{3,7},... | collective-permute-start | bytes 393224 | tf_op jit(solution)/shard_map/ppermute | solution.py:80
  145.8 3.9 %collective-permute-done.28 = bf16[128,512]{0,1:T(8,128)(2,1)S(1)} collective-permute-done((bf16[128,512]{0,1:T(8,128)(2,1)S(1)}, bf16[128,512]{0,1:T(8,128)(2,1)S(1)}, u32[]{:S(2)}, u32[]{:S(2)}) %collective-permute-start.28) | collective-permute-done | bytes 131104 | tf_op jit(solution)/shard_map/ppermute | solution.py:80
  151.1 1.7 pad_maximum_fusion.4
  156.6 21.6 %collective-permute-done.30 = bf16[128,2048]{0,1:T(8,128)(2,1)} collective-permute-done((bf16[128,2048]{0,1:T(8,128)(2,1)}, bf16[128,2048]{0,1:T(8,128)(2,1)}, u32[]{:S(2)}, u32[]{:S(2)}) %collective-permute-start.30) | collective-permute-done | bytes 524320 | tf_op jit(solution)/shard_map/ppermute | solution.py:77
  180.5 1.7 broadcast_select_fusion.1
  183.1 2.7 %reshape.621 = bf16[16,32,8,2,128]{4,3,2,1,0:T(2,128)(2,1)} reshape(bf16[16,32,2048]{2,1,0:T(8,128)(2,1)S(1)} %convolution_convert_fusion.1) | data formatting | bytes 4194304 | tf_op jit(solution)/shard_map/reshape | solution.py:241
  188.8 3.7 %broadcast_select_fusion = bf16[16,32,8,2,128]{4,3,2,1,0:T(2,128)(2,1)} fusion(bf16[16,32,8,2,128]{4,3,2,1,0:T(2,128)(2,1)S(1)} %copy-done.7, bf16[16,32,8,2,128]{4,3,2,1,0:T(2,128)(2,1)S(1)} %copy-done.2, pred[16,32]{1,0:T(8,128)(4,1)S(1)} %compare_and_fusion), kind=kLoop, calls=%fused_computation | loop fusion | flops 1048576 | bytes 6291968 | tf_op jit(solution)/shard_map/jit(_where)/select_n | solution.py:243
  (220 shorter events, 65.5 us)
Async XLA Ops:
  3.9 23.7 %collective-permute-start.23 = (bf16[128,2048]{1,0:T(8,128)(2,1)}, bf16[128,2048]{1,0:T(8,128)(2,1)}, u32[]{:S(2)}, u32[]{:S(2)}) collective-permute-start(bf16[128,2048]{1,0:T(8,128)(2,1)} %convolution_convert_fusion.2), channel_id=1, source_target_pairs={{0,2},{2,0},{4,6},{6,4},{8,10},{10,8},{12,14},{14,12},{1,3},{3,1},... | collective-permute-start | bytes 1572872 | tf_op jit(solution)/shard_map/ppermute | solution.py:77
  5.5 20.0 %collective-permute-start.5 = (f32[128]{0:T(128)S(1)}, f32[128]{0:T(128)S(1)}, u32[]{:S(2)}, u32[]{:S(2)}) collective-permute-start(f32[128]{0:T(128)S(1)} %dynamic_slice.110), channel_id=1, source_target_pairs={{0,2},{2,0},{4,6},{6,4},{8,10},{10,8},{12,14},{14,12},{1,3},{3,1},... | collective-permute-start | bytes 1544 | tf_op jit(solution)/shard_map/ppermute | solution.py:77
  8.9 22.2 %collective-permute-start.13 = (bf16[128,2048]{1,0:T(8,128)(2,1)}, bf16[128,2048]{1,0:T(8,128)(2,1)}, u32[]{:S(2)}, u32[]{:S(2)}) collective-permute-start(bf16[128,2048]{1,0:T(8,128)(2,1)} %convolution_convert_fusion.3), channel_id=1, source_target_pairs={{0,2},{2,0},{4,6},{6,4},{8,10},{10,8},{12,14},{14,12},{1,3},{3,1},... | collective-permute-start | bytes 1572872 | tf_op jit(solution)/shard_map/ppermute | solution.py:77
  11.7 28.6 %collective-permute-start.1 = (bf16[128,2048]{1,0:T(8,128)(2,1)}, bf16[128,2048]{1,0:T(8,128)(2,1)}, u32[]{:S(2)}, u32[]{:S(2)}) collective-permute-start(bf16[128,2048]{1,0:T(8,128)(2,1)} %convolution_convert_fusion.4), channel_id=1, source_target_pairs={{0,2},{2,0},{4,6},{6,4},{8,10},{10,8},{12,14},{14,12},{1,3},{3,1},... | collective-permute-start | bytes 1572872 | tf_op jit(solution)/shard_map/ppermute | solution.py:77
  25.7 9.1 %collective-permute-start.8 = (f32[128]{0:T(128)S(1)}, f32[128]{0:T(128)S(1)}, u32[]{:S(2)}, u32[]{:S(2)}) collective-permute-start(f32[128]{0:T(128)S(1)} %dynamic-slice_add_fusion), channel_id=1, source_target_pairs={{0,12},{2,14},{4,8},{6,10},{8,4},{10,6},{12,0},{14,2},{1,13},{3,15... | collective-permute-start | bytes 1544 | tf_op jit(solution)/shard_map/ppermute | solution.py:80
  25.9 16.2 %collective-permute-start.7 = (f32[128]{0:T(128)S(1)}, f32[128]{0:T(128)S(1)}, u32[]{:S(2)}, u32[]{:S(2)}) collective-permute-start(f32[128]{0:T(128)S(1)} %dynamic-slice_add_fusion), channel_id=1, source_target_pairs={{0,8},{2,10},{4,12},{6,14},{8,0},{10,2},{12,4},{14,6},{1,9},{3,11}... | collective-permute-start | bytes 1544 | tf_op jit(solution)/shard_map/ppermute | solution.py:80
  29.1 18.7 %collective-permute-start.26 = (bf16[128,512]{1,0:T(8,128)(2,1)S(1)}, bf16[128,512]{1,0:T(8,128)(2,1)S(1)}, u32[]{:S(2)}, u32[]{:S(2)}) collective-permute-start(bf16[128,512]{1,0:T(8,128)(2,1)S(1)} %get-tuple-element.18), channel_id=1, source_target_pairs={{0,12},{2,14},{4,8},{6,10},{8,4},{10,6},{12,0},{14,2},{1,13},{3,15... | collective-permute-start | bytes 393224 | tf_op jit(solution)/shard_map/ppermute | solution.py:80
  31.1 18.7 %collective-permute-start.25 = (bf16[128,512]{1,0:T(8,128)(2,1)S(1)}, bf16[128,512]{1,0:T(8,128)(2,1)S(1)}, u32[]{:S(2)}, u32[]{:S(2)}) collective-permute-start(bf16[128,512]{1,0:T(8,128)(2,1)S(1)} %get-tuple-element.19), channel_id=1, source_target_pairs={{0,8},{2,10},{4,12},{6,14},{8,0},{10,2},{12,4},{14,6},{1,9},{3,11}... | collective-permute-start | bytes 393224 | tf_op jit(solution)/shard_map/ppermute | solution.py:80
  34.7 15.4 %collective-permute-start.24 = (bf16[128,512]{1,0:T(8,128)(2,1)S(1)}, bf16[128,512]{1,0:T(8,128)(2,1)S(1)}, u32[]{:S(2)}, u32[]{:S(2)}) collective-permute-start(bf16[128,512]{1,0:T(8,128)(2,1)S(1)} %get-tuple-element.17), channel_id=1, source_target_pairs={{0,4},{2,6},{4,0},{6,2},{8,12},{10,14},{12,8},{14,10},{1,5},{3,7},... | collective-permute-start | bytes 393224 | tf_op jit(solution)/shard_map/ppermute | solution.py:80
  40.3 11.1 %collective-permute-start.16 = (bf16[128,512]{1,0:T(8,128)(2,1)S(1)}, bf16[128,512]{1,0:T(8,128)(2,1)S(1)}, u32[]{:S(2)}, u32[]{:S(2)}) collective-permute-start(bf16[128,512]{1,0:T(8,128)(2,1)S(1)} %get-tuple-element.21), channel_id=1, source_target_pairs={{0,12},{2,14},{4,8},{6,10},{8,4},{10,6},{12,0},{14,2},{1,13},{3,15... | collective-permute-start | bytes 393224 | tf_op jit(solution)/shard_map/ppermute | solution.py:80
  45.7 14.1 %collective-permute-start.15 = (bf16[128,512]{1,0:T(8,128)(2,1)S(1)}, bf16[128,512]{1,0:T(8,128)(2,1)S(1)}, u32[]{:S(2)}, u32[]{:S(2)}) collective-permute-start(bf16[128,512]{1,0:T(8,128)(2,1)S(1)} %get-tuple-element.22), channel_id=1, source_target_pairs={{0,8},{2,10},{4,12},{6,14},{8,0},{10,2},{12,4},{14,6},{1,9},{3,11}... | collective-permute-start | bytes 393224 | tf_op jit(solution)/shard_map/ppermute | solution.py:80
  47.8 13.5 %collective-permute-start.14 = (bf16[128,512]{1,0:T(8,128)(2,1)S(1)}, bf16[128,512]{1,0:T(8,128)(2,1)S(1)}, u32[]{:S(2)}, u32[]{:S(2)}) collective-permute-start(bf16[128,512]{1,0:T(8,128)(2,1)S(1)} %get-tuple-element.20), channel_id=1, source_target_pairs={{0,4},{2,6},{4,0},{6,2},{8,12},{10,14},{12,8},{14,10},{1,5},{3,7},... | collective-permute-start | bytes 393224 | tf_op jit(solution)/shard_map/ppermute | solution.py:80
  49.9 11.5 %collective-permute-start.4 = (bf16[128,512]{1,0:T(8,128)(2,1)S(1)}, bf16[128,512]{1,0:T(8,128)(2,1)S(1)}, u32[]{:S(2)}, u32[]{:S(2)}) collective-permute-start(bf16[128,512]{1,0:T(8,128)(2,1)S(1)} %get-tuple-element.24), channel_id=1, source_target_pairs={{0,12},{2,14},{4,8},{6,10},{8,4},{10,6},{12,0},{14,2},{1,13},{3,15... | collective-permute-start | bytes 393224 | tf_op jit(solution)/shard_map/ppermute | solution.py:80
  50.1 15.5 %collective-permute-start.3 = (bf16[128,512]{1,0:T(8,128)(2,1)S(1)}, bf16[128,512]{1,0:T(8,128)(2,1)S(1)}, u32[]{:S(2)}, u32[]{:S(2)}) collective-permute-start(bf16[128,512]{1,0:T(8,128)(2,1)S(1)} %get-tuple-element.25), channel_id=1, source_target_pairs={{0,8},{2,10},{4,12},{6,14},{8,0},{10,2},{12,4},{14,6},{1,9},{3,11}... | collective-permute-start | bytes 393224 | tf_op jit(solution)/shard_map/ppermute | solution.py:80
  51.4 14.2 %collective-permute-start.2 = (bf16[128,512]{1,0:T(8,128)(2,1)S(1)}, bf16[128,512]{1,0:T(8,128)(2,1)S(1)}, u32[]{:S(2)}, u32[]{:S(2)}) collective-permute-start(bf16[128,512]{1,0:T(8,128)(2,1)S(1)} %get-tuple-element.23), channel_id=1, source_target_pairs={{0,4},{2,6},{4,0},{6,2},{8,12},{10,14},{12,8},{14,10},{1,5},{3,7},... | collective-permute-start | bytes 393224 | tf_op jit(solution)/shard_map/ppermute | solution.py:80
  59.8 44.3 %collective-permute-start.12 = (bf16[8,32,8,2,128]{4,1,3,2,0:T(8,128)(2,1)}, bf16[8,32,8,2,128]{4,1,3,2,0:T(8,128)(2,1)}, u32[]{:S(2)}, u32[]{:S(2)}) collective-permute-start(bf16[8,32,8,2,128]{4,1,3,2,0:T(8,128)(2,1)} %copy.112), channel_id=1, source_target_pairs={{0,2},{2,0},{4,6},{6,4},{8,10},{10,8},{12,14},{14,12},{1,3},{3,1},... | collective-permute-start | bytes 3145736 | tf_op jit(solution)/shard_map/ppermute | solution.py:77
  67.9 21.8 %collective-permute-start.10 = (bf16[128,512]{0,1:T(8,128)(2,1)S(1)}, bf16[128,512]{0,1:T(8,128)(2,1)S(1)}, u32[]{:S(2)}, u32[]{:S(2)}) collective-permute-start(bf16[128,512]{0,1:T(8,128)(2,1)S(1)} %bitcast.271), channel_id=1, source_target_pairs={{0,8},{2,10},{4,12},{6,14},{8,0},{10,2},{12,4},{14,6},{1,9},{3,11}... | collective-permute-start | bytes 393224 | tf_op jit(solution)/shard_map/ppermute | solution.py:80
  67.9 22.6 %collective-permute-start.11 = (bf16[128,512]{0,1:T(8,128)(2,1)S(1)}, bf16[128,512]{0,1:T(8,128)(2,1)S(1)}, u32[]{:S(2)}, u32[]{:S(2)}) collective-permute-start(bf16[128,512]{0,1:T(8,128)(2,1)S(1)} %bitcast.272), channel_id=1, source_target_pairs={{0,4},{2,6},{4,0},{6,2},{8,12},{10,14},{12,8},{14,10},{1,5},{3,7},... | collective-permute-start | bytes 393224 | tf_op jit(solution)/shard_map/ppermute | solution.py:80
  72.1 20.8 %collective-permute-start.32 = (bf16[2,128,512]{2,1,0:T(8,128)(2,1)}, bf16[2,128,512]{2,1,0:T(8,128)(2,1)}, u32[]{:S(2)}, u32[]{:S(2)}) collective-permute-start(bf16[2,128,512]{2,1,0:T(8,128)(2,1)} %pad_maximum_fusion.6), channel_id=1, source_target_pairs={{0,12},{2,14},{4,8},{6,10},{8,4},{10,6},{12,0},{14,2},{1,13},{3,15... | collective-permute-start | bytes 786440 | tf_op jit(solution)/shard_map/ppermute | solution.py:80
  74.7 26.0 %collective-permute-start.33 = (bf16[2,128,512]{2,1,0:T(8,128)(2,1)}, bf16[2,128,512]{2,1,0:T(8,128)(2,1)}, u32[]{:S(2)}, u32[]{:S(2)}) collective-permute-start(bf16[2,128,512]{2,1,0:T(8,128)(2,1)} %pad_maximum_fusion.6), channel_id=1, source_target_pairs={{0,8},{2,10},{4,12},{6,14},{8,0},{10,2},{12,4},{14,6},{1,9},{3,11}... | collective-permute-start | bytes 786440 | tf_op jit(solution)/shard_map/ppermute | solution.py:80
  89.7 12.3 %collective-permute-start.34 = (bf16[2,128,512]{2,1,0:T(8,128)(2,1)}, bf16[2,128,512]{2,1,0:T(8,128)(2,1)}, u32[]{:S(2)}, u32[]{:S(2)}) collective-permute-start(bf16[2,128,512]{2,1,0:T(8,128)(2,1)} %pad_maximum_fusion.6), channel_id=1, source_target_pairs={{0,4},{2,6},{4,0},{6,2},{8,12},{10,14},{12,8},{14,10},{1,5},{3,7},... | collective-permute-start | bytes 786440 | tf_op jit(solution)/shard_map/ppermute | solution.py:80
  90.5 22.0 %collective-permute-start = (bf16[8,32,8,256]{3,1,2,0:T(8,128)(2,1)}, bf16[8,32,8,256]{3,1,2,0:T(8,128)(2,1)}, u32[]{:S(2)}, u32[]{:S(2)}) collective-permute-start(bf16[8,32,8,256]{3,1,2,0:T(8,128)(2,1)} %copy.114), channel_id=1, source_target_pairs={{0,2},{2,0},{4,6},{6,4},{8,10},{10,8},{12,14},{14,12},{1,3},{3,1},... | collective-permute-start | bytes 3145736 | tf_op jit(solution)/shard_map/ppermute | solution.py:77
  108.0 8.9 %collective-permute-start.19 = (f32[2,5,8,2,2,16]{5,4,3,2,1,0:T(2,128)S(1)}, f32[2,5,8,2,2,16]{5,4,3,2,1,0:T(2,128)S(1)}, u32[]{:S(2)}, u32[]{:S(2)}) collective-permute-start(f32[2,5,8,2,2,16]{5,4,3,2,1,0:T(2,128)S(1)} %pad_maximum_fusion.7), channel_id=1, source_target_pairs={{0,12},{2,14},{4,8},{6,10},{8,4},{10,6},{12,0},{14,2},{1,13},{3,15... | collective-permute-start | bytes 61448 | tf_op jit(solution)/shard_map/ppermute | solution.py:80
  111.0 11.6 %collective-permute-start.18 = (f32[2,5,8,2,2,16]{5,4,3,2,0,1:T(2,128)S(1)}, f32[2,5,8,2,2,16]{5,4,3,2,0,1:T(2,128)S(1)}, u32[]{:S(2)}, u32[]{:S(2)}) collective-permute-start(f32[2,5,8,2,2,16]{5,4,3,2,0,1:T(2,128)S(1)} %copy.87), channel_id=1, source_target_pairs={{0,8},{2,10},{4,12},{6,14},{8,0},{10,2},{12,4},{14,6},{1,9},{3,11}... | collective-permute-start | bytes 61448 | tf_op jit(solution)/shard_map/ppermute | solution.py:80
  111.0 11.6 %collective-permute-start.17 = (f32[2,5,8,2,2,16]{5,4,3,2,0,1:T(2,128)S(1)}, f32[2,5,8,2,2,16]{5,4,3,2,0,1:T(2,128)S(1)}, u32[]{:S(2)}, u32[]{:S(2)}) collective-permute-start(f32[2,5,8,2,2,16]{5,4,3,2,0,1:T(2,128)S(1)} %copy.87), channel_id=1, source_target_pairs={{0,4},{2,6},{4,0},{6,2},{8,12},{10,14},{12,8},{14,10},{1,5},{3,7},... | collective-permute-start | bytes 61448 | tf_op jit(solution)/shard_map/ppermute | solution.py:80
  126.7 10.0 %collective-permute-start.21 = (bf16[8,16,2,256]{3,1,2,0:T(8,128)(2,1)S(1)}, bf16[8,16,2,256]{3,1,2,0:T(8,128)(2,1)S(1)}, u32[]{:S(2)}, u32[]{:S(2)}) collective-permute-start(bf16[8,16,2,256]{3,1,2,0:T(8,128)(2,1)S(1)} %get-tuple-element.32), channel_id=1, source_target_pairs={{0,8},{2,10},{4,12},{6,14},{8,0},{10,2},{12,4},{14,6},{1,9},{3,11}... | collective-permute-start | bytes 393224 | tf_op jit(solution)/shard_map/ppermute | solution.py:80
  126.7 10.0 %collective-permute-start.20 = (bf16[8,16,2,256]{3,1,2,0:T(8,128)(2,1)S(1)}, bf16[8,16,2,256]{3,1,2,0:T(8,128)(2,1)S(1)}, u32[]{:S(2)}, u32[]{:S(2)}) collective-permute-start(bf16[8,16,2,256]{3,1,2,0:T(8,128)(2,1)S(1)} %get-tuple-element.30), channel_id=1, source_target_pairs={{0,4},{2,6},{4,0},{6,2},{8,12},{10,14},{12,8},{14,10},{1,5},{3,7},... | collective-permute-start | bytes 393224 | tf_op jit(solution)/shard_map/ppermute | solution.py:80
  139.3 10.4 %collective-permute-start.28 = (bf16[128,512]{0,1:T(8,128)(2,1)S(1)}, bf16[128,512]{0,1:T(8,128)(2,1)S(1)}, u32[]{:S(2)}, u32[]{:S(2)}) collective-permute-start(bf16[128,512]{0,1:T(8,128)(2,1)S(1)} %copy.98), channel_id=1, source_target_pairs={{0,8},{2,10},{4,12},{6,14},{8,0},{10,2},{12,4},{14,6},{1,9},{3,11}... | collective-permute-start | bytes 393224 | tf_op jit(solution)/shard_map/ppermute | solution.py:80
  139.3 10.4 %collective-permute-start.29 = (bf16[128,512]{0,1:T(8,128)(2,1)S(1)}, bf16[128,512]{0,1:T(8,128)(2,1)S(1)}, u32[]{:S(2)}, u32[]{:S(2)}) collective-permute-start(bf16[128,512]{0,1:T(8,128)(2,1)S(1)} %copy.98), channel_id=1, source_target_pairs={{0,4},{2,6},{4,0},{6,2},{8,12},{10,14},{12,8},{14,10},{1,5},{3,7},... | collective-permute-start | bytes 393224 | tf_op jit(solution)/shard_map/ppermute | solution.py:80
  143.1 37.3 %collective-permute-start.35 = (bf16[2,128,2048]{2,1,0:T(8,128)(2,1)}, bf16[2,128,2048]{2,1,0:T(8,128)(2,1)}, u32[]{:S(2)}, u32[]{:S(2)}) collective-permute-start(bf16[2,128,2048]{2,1,0:T(8,128)(2,1)} %pad_maximum_fusion.3), channel_id=1, source_target_pairs={{0,2},{2,0},{4,6},{6,4},{8,10},{10,8},{12,14},{14,12},{1,3},{3,1},... | collective-permute-start | bytes 3145736 | tf_op jit(solution)/shard_map/ppermute | solution.py:77
  152.8 25.4 %collective-permute-start.30 = (bf16[128,2048]{0,1:T(8,128)(2,1)}, bf16[128,2048]{0,1:T(8,128)(2,1)}, u32[]{:S(2)}, u32[]{:S(2)}) collective-permute-start(bf16[128,2048]{0,1:T(8,128)(2,1)} %pad_maximum_fusion.4), channel_id=1, source_target_pairs={{0,2},{2,0},{4,6},{6,4},{8,10},{10,8},{12,14},{14,12},{1,3},{3,1},... | collective-permute-start | bytes 1572872 | tf_op jit(solution)/shard_map/ppermute | solution.py:77
  180.5 13.7 %collective-permute-start.31 = (bf16[16,16,256]{2,1,0:T(8,128)(2,1)}, bf16[16,16,256]{2,1,0:T(8,128)(2,1)S(1)}, u32[]{:S(2)}, u32[]{:S(2)}) collective-permute-start(bf16[16,16,256]{2,1,0:T(8,128)(2,1)} %constant_dynamic-slice_fusion), channel_id=1, source_target_pairs={{0,1},{1,0},{2,3},{3,2},{4,5},{5,4},{6,7},{7,6},{8,9},{9,8},{10,11... | collective-permute-start | bytes 393224 | tf_op jit(solution)/shard_map/ppermute | solution.py:226
  (38 other events, 341.9 us)
